TPU v7x, 32 devices: a whole 2x2x4 slice. The times are simulated.
32 devices in a mesh: sp: 8 (over z, x), dp: 4 (over y, core).
Axes of the slice: x: 2, y: 2, z: 4, core: 2. Of those that a mesh axis runs over, the one named last changes fastest.
Arguments:
- gate_in: bfloat16 [4, 4096, 1024], P('dp', 'sp'), may hold values from -6 to 6
- value_in: bfloat16 [4, 4096, 1024], P('dp', 'sp'), may hold values from -6 to 6
- segments: int32 [4, 4096], P('dp', 'sp'), may hold values from 0 to 1, never falling along the last dimension, each value on 1 to 3072 neighbouring positions
- value_gain: bfloat16 [1024], P('sp'), may hold values from 0.099609375 to 1.8984375
- mixing: bfloat16 [8, 1024, 1024], P('sp', 'dp'), may hold values from -0.1875 to 0.1875
- mixing_bias: bfloat16 [8, 1024], P('sp'), may hold values from 0.099609375 to 1.8984375
Outputs:
- gated: bfloat16 [4, 4096, 1024], P('dp', 'sp')
Inputs may be any that keep to these rules, and one draw needn't show every extreme that they name: `segments`: within each sequence the numbers never fall, every number 0 to 1 occurs, a document spans at most 3072 positions and some document spans exactly that.
All inputs are finite; a program needn't handle non-finite values.
Results may differ from a plain program's by a relative error of at most 0.0054.
Values may be sent and summed in bfloat16 or wider, within the bound.
A program may use at most 128 MiB of HBM per device.

v0:
```python
import functools

import jax
import jax.numpy as jnp
from jax import lax
from jax.experimental import pallas as pl
from jax.experimental.pallas import tpu as pltpu
from jax.sharding import PartitionSpec as P

HEAD_DIM = 128
CORES = 2
LANES = 128
ROW_STEP = 256
PARTS = 4
MESH = pl.DeviceIdType.MESH

epsilon = 1e-06


def flip(a, b, count):
    total, bit = 0, 1
    while bit < count:
        total = total + ((a // bit + b // bit) % 2) * bit
        bit *= 2
    return total


def gelu(x):
    return jax.nn.gelu(x, approximate=True)


def to_column(row):
    parts = []
    for at in range(0, row.shape[1], LANES):
        piece = jnp.broadcast_to(row[:, at : at + LANES], (LANES, LANES))
        parts.append(piece.T)
    return jnp.concatenate(parts, axis=0)


def kernel(
    sp, dp, value_ref, ids_ref, gain_ref, mixing_ref, bias_ref, gate_ref, out_ref,
    vals, ids, mix, res, ret, bias_col, normed, ids_col, extras, extras_in,
    v_send, v_recv, i_send, i_recv, r_send, r_recv, m_send, m_recv, m_fwd, own_sem,
    e_send, e_recv, far_send, far_recv, across_send, core_send, fwd_send,
):
    s, d = lax.axis_index("sp"), lax.axis_index("dp")
    tokens = value_ref.shape[0]
    block_len = mix.shape[1]
    per = block_len // tokens
    near = sp // 2
    blocks = near // per
    rows = mixing_ref.shape[0]
    planes = dp // CORES
    half = s % per
    partner = d + 1 - 2 * (d % CORES)
    plane, core = d // CORES, d % CORES

    def across(step):
        return ((plane + step) % planes) * CORES + core

    extras[:, :block_len] = bias_ref[...].astype(jnp.float32)
    extras[:, block_len:] = gain_ref[...].astype(jnp.float32)
    barrier = pltpu.get_barrier_semaphore()
    for k in range(1, near + 1):
        pl.semaphore_signal(barrier, inc=1, device_id={"sp": flip(s, k, sp)}, device_id_type=MESH)
    pl.semaphore_signal(barrier, inc=1, device_id={"dp": partner}, device_id_type=MESH)
    for step in range(1, planes):
        pl.semaphore_signal(barrier, inc=1, device_id={"dp": across(step)}, device_id_type=MESH)
    pl.semaphore_wait(barrier, near + planes)

    def chunk(of):
        return mix.at[0, pl.ds(pl.multiple_of(of * rows, rows), rows)]

    def mix_copy(src, origin, target, sem):
        return pltpu.make_async_remote_copy(
            src_ref=src, dst_ref=chunk(origin), send_sem=sem, recv_sem=m_recv.at[origin],
            device_id={"dp": target}, device_id_type=MESH,
        )

    part = rows // PARTS

    def far_part(origin, q):
        return mix.at[1, pl.ds(pl.multiple_of(origin * rows + q * part, part), part)]

    def far_copy(src, origin, q, where, sem):
        return pltpu.make_async_remote_copy(
            src_ref=src, dst_ref=far_part(origin, q), send_sem=sem,
            recv_sem=far_recv.at[origin * PARTS + q], device_id=where, device_id_type=MESH,
        )

    def from_far(q):
        return far_copy(
            mixing_ref.at[pl.ds(q * part, part)], d, q, {"sp": flip(s, near, sp)}, far_send.at[q]
        )

    def to_plane(step, q):
        return far_copy(
            far_part(d, q), d, q, {"dp": across(step)}, across_send.at[step * PARTS + q]
        )

    def to_core(q):
        return far_copy(far_part(d, q), d, q, {"dp": partner}, core_send.at[q])

    def pass_on(step, q):
        origin = across(planes - step)
        return far_copy(
            far_part(origin, q), origin, q, {"dp": partner}, fwd_send.at[step * PARTS + q]
        )

    def extras_copy():
        return pltpu.make_async_remote_copy(
            src_ref=extras, dst_ref=extras_in, send_sem=e_send, recv_sem=e_recv,
            device_id={"sp": flip(s, near, sp)}, device_id_type=MESH,
        )

    def value_copy(k, end):
        target, head = flip(s, k % near, sp), flip(s, k, sp)
        return pltpu.make_async_remote_copy(
            src_ref=value_ref.at[:, pl.ds(pl.multiple_of(head * HEAD_DIM, HEAD_DIM), HEAD_DIM)],
            dst_ref=vals.at[k // per, pl.ds(pl.multiple_of(end * tokens, tokens), tokens)],
            send_sem=v_send.at[k], recv_sem=v_recv.at[k],
            device_id={"sp": target}, device_id_type=MESH,
        )

    def id_copy(k, end):
        return pltpu.make_async_remote_copy(
            src_ref=ids_ref, dst_ref=ids.at[k // per, end],
            send_sem=i_send.at[k], recv_sem=i_recv.at[k],
            device_id={"sp": flip(s, k, sp)}, device_id_type=MESH,
        )

    def result_copy(k):
        target = flip(s, k % near, sp)
        return pltpu.make_async_remote_copy(
            src_ref=res.at[k // per, pl.ds(pl.multiple_of((target % per) * tokens, tokens), tokens)],
            dst_ref=ret.at[k],
            send_sem=r_send.at[k], recv_sem=r_recv.at[k],
            device_id={"sp": target}, device_id_type=MESH,
        )

    for step in range(1, planes):
        mix_copy(mixing_ref, d, across(step), m_send.at[step]).start()
    mix_copy(mixing_ref, d, partner, m_send.at[0]).start()

    def send_one(k, carry):
        id_copy(k, half).start()
        value_copy(k, half).start()
        return carry

    def send_more(k, carry):
        value_copy(k, half).start()
        return carry

    extras_copy().start()
    lax.fori_loop(1, near, send_one, 0)
    for q in range(PARTS):
        from_far(q).start()
    lax.fori_loop(near + 1, sp, send_more, 0)

    own = pltpu.make_async_copy(mixing_ref, chunk(d), own_sem)
    own.start()
    for k in (0, near):
        vals[k // per, pl.ds(pl.multiple_of(half * tokens, tokens), tokens), :] = value_ref[
            :, pl.ds(pl.multiple_of(flip(s, k, sp) * HEAD_DIM, HEAD_DIM), HEAD_DIM)
        ]
    ids[0, half] = ids_ref[...]
    bias_col[0] = to_column(extras[:, :block_len])

    for step in range(1, planes):
        origin = across(planes - step)
        mix_copy(mixing_ref, origin, partner, m_send.at[0]).wait_recv()
        mix_copy(chunk(origin), origin, partner, m_fwd.at[step]).start()
    mix_copy(mixing_ref, partner, partner, m_send.at[0]).wait_recv()
    for step in range(1, planes):
        origin = across(planes - step)
        there = origin + 1 - 2 * (origin % CORES)
        mix_copy(mixing_ref, there, partner, m_send.at[0]).wait_recv()
    own.wait()

    def one_block(which, j):
        gain = (extras, extras_in)[which][:, block_len:]
        at_block = which * blocks + j
        for i in range(per):
            k = j * per + i

            @pl.when(k > 0)
            def _():
                source_half = flip(s, k, sp) % per
                if which == 0:
                    id_copy(k, source_half).wait_recv()
                value_copy(k + which * near, source_half).wait_recv()

        for at in range(0, block_len, ROW_STEP):
            act = gelu(vals[at_block, at : at + ROW_STEP, :].astype(jnp.float32))
            mean = jnp.mean(act * act, axis=-1, keepdims=True)
            normed[at : at + ROW_STEP, :] = (act * lax.rsqrt(mean + epsilon) * gain).astype(jnp.bfloat16)
        row = jnp.concatenate([ids[j, i] for i in range(per)], axis=1).astype(jnp.float32)
        ids_col[...] = to_column(row).astype(jnp.bfloat16)
        row_b = row.astype(jnp.bfloat16)
        right = normed[...]
        zero = jnp.zeros((), jnp.bfloat16)
        for at in range(0, block_len, ROW_STEP):
            col = ids_col[at : at + ROW_STEP, :]
            pieces = []
            for c in range(0, block_len, LANES):
                same = col == row_b[:, c : c + LANES]
                pieces.append(jnp.where(same, mix[which, at : at + ROW_STEP, c : c + LANES], zero))
            summed = jnp.dot(jnp.concatenate(pieces, axis=1), right, preferred_element_type=jnp.float32)
            res[at_block, at : at + ROW_STEP, :] = (summed + bias_col[which, at : at + ROW_STEP, :]).astype(jnp.bfloat16)
        for i in range(per):
            k = j * per + i

            @pl.when(k > 0)
            def _():
                result_copy(k + which * near).start()

    def relay(q):
        from_far(q).wait_recv()
        for step in range(1, planes):
            to_plane(step, q).start()
        to_core(q).start()

    def some_blocks(first, last):
        def body(j, carry):
            one_block(0, j)
            return carry

        lax.fori_loop(first, last, body, 0)

    relay(0)
    relay(1)
    some_blocks(0, blocks // 2)
    relay(2)
    some_blocks(blocks // 2, blocks)
    relay(3)
    extras_copy().wait_recv()
    bias_col[1] = to_column(extras_in[:, :block_len])
    for q in range(PARTS):
        for step in range(1, planes):
            pass_on(step, q).wait_recv()
            pass_on(step, q).start()
    for q in range(PARTS):
        far_copy(far_part(d, q), partner, q, {"dp": partner}, core_send.at[q]).wait_recv()
        for step in range(1, planes):
            origin = across(planes - step)
            there = origin + 1 - 2 * (origin % CORES)
            far_copy(far_part(d, q), there, q, {"dp": partner}, core_send.at[q]).wait_recv()

    def far_block(n, carry):
        one_block(1, blocks - 1 - n)
        return carry

    lax.fori_loop(0, blocks, far_block, 0)
    for k in (0, near):
        ret[k] = res[k // per, pl.ds(pl.multiple_of(half * tokens, tokens), tokens), :]

    def finish(k, carry):
        @pl.when(k % near > 0)
        def _():
            result_copy(k).wait_recv()

        lanes = pl.ds(pl.multiple_of(flip(s, k, sp) * HEAD_DIM, HEAD_DIM), HEAD_DIM)
        for at in range(0, tokens, ROW_STEP):
            gate = gelu(gate_ref[at : at + ROW_STEP, lanes].astype(jnp.float32))
            got = ret[k, at : at + ROW_STEP, :].astype(jnp.float32)
            out_ref[at : at + ROW_STEP, lanes] = (gate * got).astype(jnp.bfloat16)
        return carry

    lax.fori_loop(0, sp, finish, 0)

    def drain(k, carry):
        id_copy(k, half).wait_send()
        for n in (k, k + near):
            value_copy(n, half).wait_send()
            result_copy(n).wait_send()
        return carry

    lax.fori_loop(1, near, drain, 0)
    extras_copy().wait_send()
    for q in range(PARTS):
        from_far(q).wait_send()
        to_core(q).wait_send()
        for step in range(1, planes):
            to_plane(step, q).wait_send()
            pass_on(step, q).wait_send()
    mix_copy(mixing_ref, d, partner, m_send.at[0]).wait_send()
    for step in range(1, planes):
        mix_copy(mixing_ref, d, across(step), m_send.at[step]).wait_send()
        origin = across(planes - step)
        mix_copy(chunk(origin), origin, partner, m_fwd.at[step]).wait_send()


def per_device(gate_in, value_in, segments, value_gain, mixing, mixing_bias):
    sp, dp = lax.axis_size("sp"), lax.axis_size("dp")
    sequences, tokens, width = value_in.shape
    heads_here, rows, block_len = mixing.shape
    assert sequences == 1 and heads_here == 1
    per = block_len // tokens
    near = sp // 2
    blocks = near // per
    bf16, f32 = jnp.bfloat16, jnp.float32
    dma = pltpu.SemaphoreType.DMA
    vmem, anywhere = pl.BlockSpec(memory_space=pltpu.VMEM), pl.BlockSpec(memory_space=pl.ANY)
    out = pl.pallas_call(
        functools.partial(kernel, sp, dp),
        out_shape=jax.ShapeDtypeStruct((tokens, width), bf16),
        in_specs=[vmem, vmem, vmem, anywhere, vmem, vmem],
        out_specs=vmem,
        scratch_shapes=[
            pltpu.VMEM((2 * blocks, block_len, HEAD_DIM), bf16),
            pltpu.VMEM((blocks, per, 1, tokens), jnp.int32),
            pltpu.VMEM((2, block_len, block_len), bf16),
            pltpu.VMEM((2 * blocks, block_len, HEAD_DIM), bf16),
            pltpu.VMEM((sp, tokens, HEAD_DIM), bf16),
            pltpu.VMEM((2, block_len, LANES), f32),
            pltpu.VMEM((block_len, HEAD_DIM), bf16),
            pltpu.VMEM((block_len, LANES), bf16),
            pltpu.VMEM((1, block_len + HEAD_DIM), f32),
            pltpu.VMEM((1, block_len + HEAD_DIM), f32),
            dma((sp,)), dma((sp,)), dma((sp,)), dma((sp,)), dma((sp,)), dma((sp,)),
            dma((dp // CORES,)), dma((dp,)), dma((dp // CORES,)), dma,
            dma, dma, dma((PARTS,)), dma((dp * PARTS,)), dma((dp // CORES * PARTS,)),
            dma((PARTS,)), dma((dp // CORES * PARTS,)),
        ],
        compiler_params=pltpu.CompilerParams(
            collective_id=0, has_side_effects=True, vmem_limit_bytes=60 * 1024 * 1024
        ),
    )(
        value_in.reshape(tokens, width),
        segments,
        value_gain.reshape(1, HEAD_DIM),
        mixing.reshape(rows, block_len),
        mixing_bias,
        gate_in.reshape(tokens, width),
    )
    return out.reshape(sequences, tokens, width)


def solution(mesh):
    return jax.shard_map(
        per_device,
        mesh=mesh,
        in_specs=(
            P("dp", "sp", None),
            P("dp", "sp", None),
            P("dp", "sp"),
            P("sp"),
            P("sp", "dp", None),
            P("sp", None),
        ),
        out_specs=P("dp", "sp", None),
        check_vma=False,
    )
```

profile of v0, /device:TPU:0, one launch (start us, length us, event | category | flops | bytes accessed | tf_op | source)
XLA Modules:
  0.0 50.2 jit_solution(1900856004259756125)
XLA Ops:
  0.0 47.9 %shard_map.64 = bf16[512,1024]{1,0:T(8,128)(2,1)} custom-call(bf16[512,1024]{1,0:T(8,128)(2,1)} %bitcast.6, s32[1,512]{1,0:T(1,128)} %ids_ref.1, bf16[1,128]{1,0:T(2,128)(2,1)} %bitcast.9, bf16[256,1024]{1,0:T(8,128)(2,1)} %bitcast.8, bf16[1,1024]{1,0:T(2,128)(2,1)} %bias_ref.1, bf16[512,1024]{1,0:T(8,128)(2,1)} %bitcast.7), custom_call_target="tpu_custom_call" | custom-call | tf_op jit(solution)/shard_map/pallas_call | solution.py:304
  47.9 2.3 %copy.8 = bf16[1,512,1024]{2,1,0:T(8,128)(2,1)} copy(bf16[1,512,1024]{2,1,0:T(8,128)(2,1)} %bitcast.5) | data formatting | bytes 2097152
where the time goes:
time: 50.4 us; the launch traced here: 50.2 us
  Pallas kernels  47.9 us (95%)
  local copies, waits for them, and re-layouts  2.26 us (4%)
    pallas_call x1, Pallas kernels, per_device(): pl.pallas_call(functools.partial(kernel, sp, dp), out_shape=jax.ShapeDtyp...  47.9 us
    unnamed x1, local copies, waits for them, and re-layouts  2.26 us

commit v1 on v0

v1 whole, which is shorter than its diff:
```python
import functools

import jax
import jax.numpy as jnp
from jax import lax
from jax.experimental import pallas as pl
from jax.experimental.pallas import tpu as pltpu
from jax.sharding import PartitionSpec as P

HEAD_DIM = 128
CORES = 2
LANES = 128
ROW_STEP = 256
PARTS = 4
MESH = pl.DeviceIdType.MESH

epsilon = 1e-06


def flip(a, b, count):
    total, bit = 0, 1
    while bit < count:
        total = total + ((a // bit + b // bit) % 2) * bit
        bit *= 2
    return total


def gelu(x):
    return jax.nn.gelu(x, approximate=True)


def to_column(row):
    parts = []
    for at in range(0, row.shape[1], LANES):
        piece = jnp.broadcast_to(row[:, at : at + LANES], (LANES, LANES))
        parts.append(piece.T)
    return jnp.concatenate(parts, axis=0)


def kernel(
    sp, dp, value_hbm, ids_hbm, gain_hbm, mixing_ref, bias_hbm, gate_hbm, out_ref,
    value_ref, gate_ref, ids_ref, gain_ref, bias_ref,
    act_gate, vals, normed, ids, ids_row, ids_col, mix, res, ret, bias_col, extras, extras_in,
    in_sem, v_send, v_recv, i_send, i_recv, r_send, r_recv,
    mix_recv, across_send, core_send, fwd_send, own_sem, far_send, e_send, e_recv, far_ok,
):
    s, d = lax.axis_index("sp"), lax.axis_index("dp")
    tokens = value_ref.shape[0]
    block_len = mix.shape[1]
    per = block_len // tokens
    near = sp // 2
    blocks = near // per
    rows = mixing_ref.shape[0]
    part = rows // PARTS
    planes = dp // CORES
    half = s % per
    partner = d + 1 - 2 * (d % CORES)
    plane, core = d // CORES, d % CORES
    each = dp // per
    far = flip(s, sp - per, sp)
    level, levels = s // per, sp // per
    mid = (level == levels // 2 - 1) | (level == levels // 2)
    outer = (level < levels // 2 - 1) | (level > levels // 2)

    def across(step):
        return ((plane + step) % planes) * CORES + core

    barrier = pltpu.get_barrier_semaphore()
    for k in range(1, near):
        pl.semaphore_signal(barrier, inc=1, device_id={"sp": flip(s, k, sp)}, device_id_type=MESH)
    pl.semaphore_signal(barrier, inc=1, device_id={"dp": partner}, device_id_type=MESH)
    for step in range(1, planes):
        pl.semaphore_signal(barrier, inc=1, device_id={"dp": across(step)}, device_id_type=MESH)

    @pl.when(mid)
    def _():
        pl.semaphore_signal(barrier, inc=1, device_id={"sp": far}, device_id_type=MESH)

    loads = [
        pltpu.make_async_copy(src, dst, in_sem.at[n])
        for n, (src, dst) in enumerate([
            (value_hbm, value_ref), (ids_hbm, ids_ref), (gain_hbm, gain_ref),
            (bias_hbm, bias_ref), (gate_hbm, gate_ref),
        ])
    ]
    for load in loads:
        load.start()

    def chunk(which, origin, q):
        return mix.at[which, pl.ds(pl.multiple_of(origin * rows + q * part, part), part)]

    def part_copy(which, src, origin, q, where, sem):
        return pltpu.make_async_remote_copy(
            src_ref=src, dst_ref=chunk(which, origin, q), send_sem=sem,
            recv_sem=mix_recv.at[(which * dp + origin) * PARTS + q],
            device_id=where, device_id_type=MESH,
        )

    def held(which, q):
        return chunk(1, d, q) if which else mixing_ref.at[pl.ds(q * part, part)]

    def from_far(q):
        return part_copy(1, mixing_ref.at[pl.ds(q * part, part)], d, q, {"sp": far}, far_send.at[q])

    def to_plane(which, step, q):
        sem = across_send.at[(which * planes + step) * PARTS + q]
        return part_copy(which, held(which, q), d, q, {"dp": across(step)}, sem)

    def to_core(which, q):
        return part_copy(which, held(which, q), d, q, {"dp": partner}, core_send.at[which * PARTS + q])

    def pass_on(which, step, q):
        origin = across(planes - step)
        sem = fwd_send.at[(which * planes + step) * PARTS + q]
        return part_copy(which, chunk(which, origin, q), origin, q, {"dp": partner}, sem)

    def share(which, q):
        for step in range(1, planes):
            to_plane(which, step, q).start()
        to_core(which, q).start()

    def forward(which, q):
        for step in range(1, planes):
            pass_on(which, step, q).wait_recv()
            pass_on(which, step, q).start()

    def arrived(which, q):
        part_copy(which, held(which, q), partner, q, {"dp": partner}, core_send.at[0]).wait_recv()
        for step in range(1, planes):
            origin = across(planes - step)
            there = origin + 1 - 2 * (origin % CORES)
            part_copy(which, held(which, q), there, q, {"dp": partner}, core_send.at[0]).wait_recv()

    def extras_copy():
        return pltpu.make_async_remote_copy(
            src_ref=extras, dst_ref=extras_in, send_sem=e_send, recv_sem=e_recv,
            device_id={"sp": far}, device_id_type=MESH,
        )

    def head_of(owner, which):
        return flip(owner, which * (sp - per), sp)

    def lanes_of(head):
        return pl.ds(pl.multiple_of(head * HEAD_DIM, HEAD_DIM), HEAD_DIM)

    def value_copy(which, k, end):
        target = flip(s, k, sp)
        return pltpu.make_async_remote_copy(
            src_ref=value_ref.at[:, lanes_of(head_of(target, which))],
            dst_ref=vals.at[which * blocks + k // per, pl.ds(pl.multiple_of(end * tokens, tokens), tokens)],
            send_sem=v_send.at[which * near + k], recv_sem=v_recv.at[which * near + k],
            device_id={"sp": target}, device_id_type=MESH,
        )

    def id_copy(k, end):
        return pltpu.make_async_remote_copy(
            src_ref=ids_ref, dst_ref=ids.at[k // per, end],
            send_sem=i_send.at[k], recv_sem=i_recv.at[k],
            device_id={"sp": flip(s, k, sp)}, device_id_type=MESH,
        )

    def result_copy(which, k, q):
        target = flip(s, k, sp)
        at = (which * near + k) * PARTS + q
        return pltpu.make_async_remote_copy(
            src_ref=res.at[which * blocks + k // per, q, pl.ds((target % per) * each, each)],
            dst_ref=ret.at[which * near + k, q],
            send_sem=r_send.at[at], recv_sem=r_recv.at[at],
            device_id={"sp": target}, device_id_type=MESH,
        )

    pl.semaphore_wait(barrier, near - 1 + planes + mid.astype(jnp.int32))

    @pl.when(mid)
    def _():
        pl.semaphore_signal(far_ok, inc=1, device_id={"sp": far}, device_id_type=MESH)
        for q in range(PARTS):
            from_far(q).start()

    for q in range(PARTS):
        share(0, q)
    own = [pltpu.make_async_copy(mixing_ref.at[pl.ds(q * part, part)], chunk(0, d, q), own_sem.at[q]) for q in range(PARTS)]
    for copy in own:
        copy.start()
    loads[0].wait()
    loads[1].wait()

    def send_one(k, carry):
        value_copy(0, k, half).start()
        id_copy(k, half).start()
        return carry

    def send_more(k, carry):
        value_copy(1, k, half).start()
        return carry

    lax.fori_loop(1, near, send_one, 0)
    lax.fori_loop(1, near, send_more, 0)
    loads[2].wait()
    loads[3].wait()
    extras[:, :block_len] = bias_ref[...].astype(jnp.float32)
    extras[:, block_len:] = gain_ref[...].astype(jnp.float32)
    for which in (0, 1):
        vals[which * blocks, pl.ds(pl.multiple_of(half * tokens, tokens), tokens), :] = value_ref[:, lanes_of(head_of(s, which))]
    ids[0, half] = ids_ref[...]
    bias_col[0] = to_column(extras[:, :block_len])

    @pl.when(mid)
    def _():
        pl.semaphore_wait(far_ok, 1)
        for k in range(per, near, per):
            pl.semaphore_signal(far_ok, inc=1, device_id={"sp": flip(s, k, sp)}, device_id_type=MESH)
        extras_copy().start()

    @pl.when(outer)
    def _():
        pl.semaphore_wait(far_ok, 1)
        for q in range(PARTS):
            from_far(q).start()
        extras_copy().start()

    loads[4].wait()

    def gate_rows(n, carry):
        at = pl.ds(pl.multiple_of(n * LANES, LANES), LANES)
        act_gate[at, :] = gelu(gate_ref[at, :].astype(jnp.float32))
        return carry

    lax.fori_loop(0, tokens // LANES, gate_rows, 0)

    def norm_block(which, j):
        gain = (extras, extras_in)[which][:, block_len:]
        for i in range(per):
            k = j * per + i

            @pl.when(k > 0)
            def _():
                source_half = flip(s, k, sp) % per
                if which == 0:
                    id_copy(k, source_half).wait_recv()
                value_copy(which, k, source_half).wait_recv()

        n = which * blocks + j
        for at in range(0, block_len, ROW_STEP):
            act = gelu(vals[n, at : at + ROW_STEP, :].astype(jnp.float32))
            mean = jnp.mean(act * act, axis=-1, keepdims=True)
            normed[n, at : at + ROW_STEP, :] = (act * lax.rsqrt(mean + epsilon) * gain).astype(jnp.bfloat16)
        if which == 0:
            row = jnp.concatenate([ids[j, i] for i in range(per)], axis=1).astype(jnp.float32)
            ids_row[j] = row
            ids_col[j] = to_column(row).astype(jnp.bfloat16)

    def norm_blocks(which, first, last):
        def body(j, carry):
            norm_block(which, j)
            return carry

        lax.fori_loop(first, last, body, 0)

    zero = jnp.zeros((), jnp.bfloat16)

    def mix_part(which, q):
        def body(j, carry):
            n = which * blocks + j
            row_b = ids_row[j].astype(jnp.bfloat16)
            right = normed[n]
            tall = []
            for origin in range(dp):
                at = origin * rows + q * part
                col = ids_col[j, pl.ds(pl.multiple_of(at, part), part), :]
                wide = []
                for c in range(0, block_len, LANES):
                    same = col == row_b[:, c : c + LANES]
                    piece = mix[which, pl.ds(pl.multiple_of(at, part), part), c : c + LANES]
                    wide.append(jnp.where(same, piece, zero))
                tall.append(jnp.concatenate(wide, axis=1))
            summed = jnp.dot(jnp.concatenate(tall, axis=0), right, preferred_element_type=jnp.float32)
            for origin in range(dp):
                at = origin * rows + q * part
                bias = bias_col[which, pl.ds(pl.multiple_of(at, part), part), :]
                res[n, q, origin] = (summed[origin * part : (origin + 1) * part] + bias).astype(jnp.bfloat16)
            for i in range(per):
                k = j * per + i

                @pl.when(k > 0)
                def _():
                    result_copy(which, k, q).start()
            return carry

        lax.fori_loop(0, blocks, body, 0)

    forward(0, 0)
    norm_blocks(0, 0, blocks // 2)
    forward(0, 1)
    norm_blocks(0, blocks // 2, blocks)
    forward(0, 2)
    extras_copy().wait_recv()
    bias_col[1] = to_column(extras_in[:, :block_len])
    norm_blocks(1, 0, blocks // 2)
    forward(0, 3)
    norm_blocks(1, blocks // 2, blocks)

    def relay(q):
        from_far(q).wait_recv()
        share(1, q)

    @pl.when(mid)
    def _():
        for q in range(PARTS):
            relay(q)

    for q in range(PARTS):
        own[q].wait()
        arrived(0, q)
        mix_part(0, q)

    for n in range(PARTS + 2):
        if n < PARTS:
            @pl.when(outer)
            def _():
                relay(n)
        if n >= 2:
            arrived(1, n - 2)
            mix_part(1, n - 2)
        if 1 <= n < PARTS + 1:
            forward(1, n - 1)

    def finish_one(which, k, source, n):
        lanes = lanes_of(head_of(flip(s, k, sp), which))
        for q in range(PARTS):
            for e in range(each):
                at = e * rows + q * part
                got = source(q, e).astype(jnp.float32)
                out_ref[at : at + part, lanes] = (act_gate[at : at + part, lanes] * got).astype(jnp.bfloat16)

    for which in (0, 1):
        finish_one(which, 0, lambda q, e: res[which * blocks, q, half * each + e], 0)

        def finish(k, carry):
            for q in range(PARTS):
                result_copy(which, k, q).wait_recv()
            finish_one(which, k, lambda q, e: ret[which * near + k, q, e], 0)
            return carry

        lax.fori_loop(1, near, finish, 0)

    def drain(k, carry):
        id_copy(k, half).wait_send()
        for which in (0, 1):
            value_copy(which, k, half).wait_send()
            for q in range(PARTS):
                result_copy(which, k, q).wait_send()
        return carry

    lax.fori_loop(1, near, drain, 0)
    extras_copy().wait_send()
    for q in range(PARTS):
        from_far(q).wait_send()
        for which in (0, 1):
            to_core(which, q).wait_send()
            for step in range(1, planes):
                to_plane(which, step, q).wait_send()
                pass_on(which, step, q).wait_send()


def per_device(gate_in, value_in, segments, value_gain, mixing, mixing_bias):
    sp, dp = lax.axis_size("sp"), lax.axis_size("dp")
    sequences, tokens, width = value_in.shape
    heads_here, rows, block_len = mixing.shape
    assert sequences == 1 and heads_here == 1
    per = block_len // tokens
    near = sp // 2
    blocks = near // per
    planes = dp // CORES
    part = rows // PARTS
    bf16, f32 = jnp.bfloat16, jnp.float32
    dma = pltpu.SemaphoreType.DMA
    vmem, anywhere = pl.BlockSpec(memory_space=pltpu.VMEM), pl.BlockSpec(memory_space=pl.ANY)
    out = pl.pallas_call(
        functools.partial(kernel, sp, dp),
        out_shape=jax.ShapeDtypeStruct((tokens, width), bf16),
        in_specs=[anywhere] * 6,
        out_specs=vmem,
        scratch_shapes=[
            pltpu.VMEM((tokens, width), bf16),
            pltpu.VMEM((tokens, width), bf16),
            pltpu.VMEM((1, tokens), jnp.int32),
            pltpu.VMEM((1, HEAD_DIM), bf16),
            pltpu.VMEM((1, block_len), bf16),
            pltpu.VMEM((tokens, width), f32),
            pltpu.VMEM((2 * blocks, block_len, HEAD_DIM), bf16),
            pltpu.VMEM((2 * blocks, block_len, HEAD_DIM), bf16),
            pltpu.VMEM((blocks, per, 1, tokens), jnp.int32),
            pltpu.VMEM((blocks, 1, block_len), f32),
            pltpu.VMEM((blocks, block_len, LANES), bf16),
            pltpu.VMEM((2, block_len, block_len), bf16),
            pltpu.VMEM((2 * blocks, PARTS, dp, part, HEAD_DIM), bf16),
            pltpu.VMEM((sp, PARTS, dp // per, part, HEAD_DIM), bf16),
            pltpu.VMEM((2, block_len, LANES), f32),
            pltpu.VMEM((1, block_len + HEAD_DIM), f32),
            pltpu.VMEM((1, block_len + HEAD_DIM), f32),
            dma((5,)), dma((sp,)), dma((sp,)), dma((sp,)), dma((sp,)),
            dma((sp * PARTS,)), dma((sp * PARTS,)),
            dma((2 * dp * PARTS,)), dma((2 * planes * PARTS,)), dma((2 * PARTS,)),
            dma((2 * planes * PARTS,)), dma((PARTS,)), dma((PARTS,)), dma, dma,
            pltpu.SemaphoreType.REGULAR,
        ],
        compiler_params=pltpu.CompilerParams(
            collective_id=0, has_side_effects=True, vmem_limit_bytes=60 * 1024 * 1024
        ),
    )(
        value_in.reshape(tokens, width),
        segments,
        value_gain.reshape(1, HEAD_DIM),
        mixing.reshape(rows, block_len),
        mixing_bias,
        gate_in.reshape(tokens, width),
    )
    return out.reshape(sequences, tokens, width)


def solution(mesh):
    return jax.shard_map(
        per_device,
        mesh=mesh,
        in_specs=(
            P("dp", "sp", None),
            P("dp", "sp", None),
            P("dp", "sp"),
            P("sp"),
            P("sp", "dp", None),
            P("sp", None),
        ),
        out_specs=P("dp", "sp", None),
        check_vma=False,
    )
```

time: 50.4 us -> 56 us (1.11)
  Pallas kernels: 47.9 us -> 53.6 us
    pallas_call x1, Pallas kernels: 47.9 us -> 53.6 us  [per_device(): pl.pallas_call(functools.partial(kernel, sp, dp), out_shape=jax.ShapeDtyp...]
where the time goes in v1:
time: 56 us; the launch traced here: 55.8 us
  Pallas kernels  53.6 us (96%)
  local copies, waits for them, and re-layouts  2.26 us (4%)
    pallas_call x1, Pallas kernels, per_device(): pl.pallas_call(functools.partial(kernel, sp, dp), out_shape=jax.ShapeDtyp...  53.6 us
    unnamed x1, local copies, waits for them, and re-layouts  2.26 us

profile of v1, /device:TPU:0, one launch (start us, length us, event | category | flops | bytes accessed | tf_op | source)
XLA Modules:
  0.0 55.8 jit_solution(453251200779425151)
XLA Ops:
  0.0 53.6 %shard_map.64 = bf16[512,1024]{1,0:T(8,128)(2,1)} custom-call(bf16[512,1024]{1,0:T(8,128)(2,1)} %bitcast.6, s32[1,512]{1,0:T(1,128)} %ids_hbm.1, bf16[1,128]{1,0:T(2,128)(2,1)} %bitcast.9, bf16[256,1024]{1,0:T(8,128)(2,1)} %bitcast.8, bf16[1,1024]{1,0:T(2,128)(2,1)} %bias_hbm.1, bf16[512,1024]{1,0:T(8,128)(2,1)} %bitcast.7), custom_call_target="tpu_custom_call" | custom-call | tf_op jit(solution)/shard_map/pallas_call | solution.py:379
  53.6 2.3 %copy.8 = bf16[1,512,1024]{2,1,0:T(8,128)(2,1)} copy(bf16[1,512,1024]{2,1,0:T(8,128)(2,1)} %bitcast.5) | data formatting | bytes 2097152

commit v2 on v1

--- a/solution.py
+++ b/solution.py
@@ -86,8 +86,11 @@
     for load in loads:
         load.start()
 
+    count = (1, PARTS)
+
     def chunk(which, origin, q):
-        return mix.at[which, pl.ds(pl.multiple_of(origin * rows + q * part, part), part)]
+        size = rows // count[which]
+        return mix.at[which, pl.ds(pl.multiple_of(origin * rows + q * size, size), size)]
 
     def part_copy(which, src, origin, q, where, sem):
         return pltpu.make_async_remote_copy(
@@ -97,7 +100,7 @@
         )
 
     def held(which, q):
-        return chunk(1, d, q) if which else mixing_ref.at[pl.ds(q * part, part)]
+        return chunk(1, d, q) if which else mixing_ref
 
     def from_far(q):
         return part_copy(1, mixing_ref.at[pl.ds(q * part, part)], d, q, {"sp": far}, far_send.at[q])
@@ -169,19 +172,22 @@
             device_id={"sp": target}, device_id_type=MESH,
         )
 
+    loads[2].wait()
+    loads[3].wait()
+    extras[:, :block_len] = bias_ref[...].astype(jnp.float32)
+    extras[:, block_len:] = gain_ref[...].astype(jnp.float32)
     pl.semaphore_wait(barrier, near - 1 + planes + mid.astype(jnp.int32))
 
     @pl.when(mid)
     def _():
         pl.semaphore_signal(far_ok, inc=1, device_id={"sp": far}, device_id_type=MESH)
+        extras_copy().start()
         for q in range(PARTS):
             from_far(q).start()
 
-    for q in range(PARTS):
-        share(0, q)
-    own = [pltpu.make_async_copy(mixing_ref.at[pl.ds(q * part, part)], chunk(0, d, q), own_sem.at[q]) for q in range(PARTS)]
-    for copy in own:
-        copy.start()
+    share(0, 0)
+    own = pltpu.make_async_copy(mixing_ref, chunk(0, d, 0), own_sem)
+    own.start()
     loads[0].wait()
     loads[1].wait()
 
@@ -196,10 +202,6 @@
 
     lax.fori_loop(1, near, send_one, 0)
     lax.fori_loop(1, near, send_more, 0)
-    loads[2].wait()
-    loads[3].wait()
-    extras[:, :block_len] = bias_ref[...].astype(jnp.float32)
-    extras[:, block_len:] = gain_ref[...].astype(jnp.float32)
     for which in (0, 1):
         vals[which * blocks, pl.ds(pl.multiple_of(half * tokens, tokens), tokens), :] = value_ref[:, lanes_of(head_of(s, which))]
     ids[0, half] = ids_ref[...]
@@ -210,14 +212,13 @@
         pl.semaphore_wait(far_ok, 1)
         for k in range(per, near, per):
             pl.semaphore_signal(far_ok, inc=1, device_id={"sp": flip(s, k, sp)}, device_id_type=MESH)
-        extras_copy().start()
 
     @pl.when(outer)
     def _():
         pl.semaphore_wait(far_ok, 1)
+        extras_copy().start()
         for q in range(PARTS):
             from_far(q).start()
-        extras_copy().start()
 
     loads[4].wait()
 
@@ -289,16 +290,7 @@
 
         lax.fori_loop(0, blocks, body, 0)
 
-    forward(0, 0)
-    norm_blocks(0, 0, blocks // 2)
-    forward(0, 1)
-    norm_blocks(0, blocks // 2, blocks)
-    forward(0, 2)
-    extras_copy().wait_recv()
-    bias_col[1] = to_column(extras_in[:, :block_len])
-    norm_blocks(1, 0, blocks // 2)
-    forward(0, 3)
-    norm_blocks(1, blocks // 2, blocks)
+    norm_blocks(0, 0, blocks)
 
     def relay(q):
         from_far(q).wait_recv()
@@ -309,9 +301,10 @@
         for q in range(PARTS):
             relay(q)
 
+    forward(0, 0)
+    own.wait()
+    arrived(0, 0)
     for q in range(PARTS):
-        own[q].wait()
-        arrived(0, q)
         mix_part(0, q)
 
     for n in range(PARTS + 2):
@@ -319,6 +312,10 @@
             @pl.when(outer)
             def _():
                 relay(n)
+        if n == 0:
+            extras_copy().wait_recv()
+            bias_col[1] = to_column(extras_in[:, :block_len])
+            norm_blocks(1, 0, blocks)
         if n >= 2:
             arrived(1, n - 2)
             mix_part(1, n - 2)
@@ -356,7 +353,8 @@
     extras_copy().wait_send()
     for q in range(PARTS):
         from_far(q).wait_send()
-        for which in (0, 1):
+    for which in (0, 1):
+        for q in range(count[which]):
             to_core(which, q).wait_send()
             for step in range(1, planes):
                 to_plane(which, step, q).wait_send()
@@ -402,7 +400,7 @@
             dma((5,)), dma((sp,)), dma((sp,)), dma((sp,)), dma((sp,)),
             dma((sp * PARTS,)), dma((sp * PARTS,)),
             dma((2 * dp * PARTS,)), dma((2 * planes * PARTS,)), dma((2 * PARTS,)),
-            dma((2 * planes * PARTS,)), dma((PARTS,)), dma((PARTS,)), dma, dma,
+            dma((2 * planes * PARTS,)), dma, dma((PARTS,)), dma, dma,
             pltpu.SemaphoreType.REGULAR,
         ],
         compiler_params=pltpu.CompilerParams(

time: 56 us -> 47.5 us (0.85)
  Pallas kernels: 53.6 us -> 45 us
    pallas_call x1, Pallas kernels: 53.6 us -> 45 us  [per_device(): pl.pallas_call(functools.partial(kernel, sp, dp), out_shape=jax.ShapeDtyp...]
where the time goes in v2:
time: 47.5 us; the launch traced here: 47.3 us
  Pallas kernels  45 us (95%)
  local copies, waits for them, and re-layouts  2.26 us (5%)
    pallas_call x1, Pallas kernels, per_device(): pl.pallas_call(functools.partial(kernel, sp, dp), out_shape=jax.ShapeDtyp...  45 us
    unnamed x1, local copies, waits for them, and re-layouts  2.26 us

profile of v2, /device:TPU:0, one launch (start us, length us, event | category | flops | bytes accessed | tf_op | source)
XLA Modules:
  0.0 47.3 jit_solution(13164732963740017320)
XLA Ops:
  0.0 45.0 %shard_map.64 = bf16[512,1024]{1,0:T(8,128)(2,1)} custom-call(bf16[512,1024]{1,0:T(8,128)(2,1)} %bitcast.6, s32[1,512]{1,0:T(1,128)} %ids_hbm.1, bf16[1,128]{1,0:T(2,128)(2,1)} %bitcast.9, bf16[256,1024]{1,0:T(8,128)(2,1)} %bitcast.8, bf16[1,1024]{1,0:T(2,128)(2,1)} %bias_hbm.1, bf16[512,1024]{1,0:T(8,128)(2,1)} %bitcast.7), custom_call_target="tpu_custom_call" | custom-call | tf_op jit(solution)/shard_map/pallas_call | solution.py:377
  45.0 2.3 %copy.8 = bf16[1,512,1024]{2,1,0:T(8,128)(2,1)} copy(bf16[1,512,1024]{2,1,0:T(8,128)(2,1)} %bitcast.5) | data formatting | bytes 2097152

commit v3 on v2

--- a/solution.py
+++ b/solution.py
@@ -38,11 +38,11 @@
 
 
 def kernel(
-    sp, dp, value_hbm, ids_hbm, gain_hbm, mixing_ref, bias_hbm, gate_hbm, out_ref,
-    value_ref, gate_ref, ids_ref, gain_ref, bias_ref,
-    act_gate, vals, normed, ids, ids_row, ids_col, mix, res, ret, bias_col, extras, extras_in,
+    sp, dp, value_hbm, ids_hbm, gain_hbm, mixing_ref, bias_hbm, mixed_ref,
+    value_ref, ids_ref, gain_ref, bias_ref,
+    vals, normed, ids, ids_row, ids_col, mix, res, bias_col, extras, extras_in,
     in_sem, v_send, v_recv, i_send, i_recv, r_send, r_recv,
-    mix_recv, across_send, core_send, fwd_send, own_sem, far_send, e_send, e_recv, far_ok,
+    mix_recv, across_send, core_send, fwd_send, own_sem, far_send, e_send, e_recv, far_ok, keep_sem,
 ):
     s, d = lax.axis_index("sp"), lax.axis_index("dp")
     tokens = value_ref.shape[0]
@@ -80,7 +80,7 @@
         pltpu.make_async_copy(src, dst, in_sem.at[n])
         for n, (src, dst) in enumerate([
             (value_hbm, value_ref), (ids_hbm, ids_ref), (gain_hbm, gain_ref),
-            (bias_hbm, bias_ref), (gate_hbm, gate_ref),
+            (bias_hbm, bias_ref),
         ])
     ]
     for load in loads:
@@ -162,12 +162,21 @@
             device_id={"sp": flip(s, k, sp)}, device_id_type=MESH,
         )
 
+    def place(owner, which, q):
+        return mixed_ref.at[:, q, :, lanes_of(head_of(owner, which))]
+
+    def keep_copy(which, q):
+        return pltpu.make_async_copy(
+            res.at[which * blocks, q, pl.ds(half * each, each)],
+            place(s, which, q), keep_sem.at[which * PARTS + q],
+        )
+
     def result_copy(which, k, q):
         target = flip(s, k, sp)
         at = (which * near + k) * PARTS + q
         return pltpu.make_async_remote_copy(
             src_ref=res.at[which * blocks + k // per, q, pl.ds((target % per) * each, each)],
-            dst_ref=ret.at[which * near + k, q],
+            dst_ref=place(s, which, q),
             send_sem=r_send.at[at], recv_sem=r_recv.at[at],
             device_id={"sp": target}, device_id_type=MESH,
         )
@@ -219,15 +228,6 @@
         extras_copy().start()
         for q in range(PARTS):
             from_far(q).start()
-
-    loads[4].wait()
-
-    def gate_rows(n, carry):
-        at = pl.ds(pl.multiple_of(n * LANES, LANES), LANES)
-        act_gate[at, :] = gelu(gate_ref[at, :].astype(jnp.float32))
-        return carry
-
-    lax.fori_loop(0, tokens // LANES, gate_rows, 0)
 
     def norm_block(which, j):
         gain = (extras, extras_in)[which][:, block_len:]
@@ -260,8 +260,9 @@
 
     zero = jnp.zeros((), jnp.bfloat16)
 
-    def mix_part(which, q):
-        def body(j, carry):
+    def mix_part(which, q, first=0, last=blocks):
+        def body(m, carry):
+            j = last - 1 - m
             n = which * blocks + j
             row_b = ids_row[j].astype(jnp.bfloat16)
             right = normed[n]
@@ -286,9 +287,13 @@
                 @pl.when(k > 0)
                 def _():
                     result_copy(which, k, q).start()
+
+                @pl.when(k == 0)
+                def _():
+                    keep_copy(which, q).start()
             return carry
 
-        lax.fori_loop(0, blocks, body, 0)
+        lax.fori_loop(0, last - first, body, 0)
 
     norm_blocks(0, 0, blocks)
 
@@ -296,50 +301,67 @@
         from_far(q).wait_recv()
         share(1, q)
 
+    def near_parts(first, last):
+        def body(q, carry):
+            mix_part(0, q, first, last)
+            return carry
+
+        lax.fori_loop(0, PARTS, body, 0)
+
+    def near_here():
+        forward(0, 0)
+        own.wait()
+        arrived(0, 0)
+        near_parts(0, blocks)
+
+    def far_values():
+        extras_copy().wait_recv()
+        bias_col[1] = to_column(extras_in[:, :block_len])
+        norm_blocks(1, 0, blocks)
+
+    def far_part(q):
+        arrived(1, q)
+        mix_part(1, q)
+
     @pl.when(mid)
     def _():
+        relay(0)
+        relay(1)
+        near_here()
+        far_values()
         for q in range(PARTS):
+            forward(1, q)
+            if q + 2 < PARTS:
+                relay(q + 2)
+            if q > 0:
+                far_part(q - 1)
+        far_part(PARTS - 1)
+
+    @pl.when(outer)
+    def _():
+        near_here()
+        relay(0)
+        far_values()
+        relay(1)
+        forward(1, 0)
+        for q in range(2, PARTS):
             relay(q)
-
-    forward(0, 0)
-    own.wait()
-    arrived(0, 0)
-    for q in range(PARTS):
-        mix_part(0, q)
-
-    for n in range(PARTS + 2):
-        if n < PARTS:
-            @pl.when(outer)
-            def _():
-                relay(n)
-        if n == 0:
-            extras_copy().wait_recv()
-            bias_col[1] = to_column(extras_in[:, :block_len])
-            norm_blocks(1, 0, blocks)
-        if n >= 2:
-            arrived(1, n - 2)
-            mix_part(1, n - 2)
-        if 1 <= n < PARTS + 1:
-            forward(1, n - 1)
-
-    def finish_one(which, k, source, n):
-        lanes = lanes_of(head_of(flip(s, k, sp), which))
+            forward(1, q - 1)
+            far_part(q - 2)
+        far_part(PARTS - 2)
+        forward(1, PARTS - 1)
+        far_part(PARTS - 1)
+
+    for which in (0, 1):
         for q in range(PARTS):
-            for e in range(each):
-                at = e * rows + q * part
-                got = source(q, e).astype(jnp.float32)
-                out_ref[at : at + part, lanes] = (act_gate[at : at + part, lanes] * got).astype(jnp.bfloat16)
-
-    for which in (0, 1):
-        finish_one(which, 0, lambda q, e: res[which * blocks, q, half * each + e], 0)
-
-        def finish(k, carry):
+            keep_copy(which, q).wait()
+
+        def collect(k, carry):
             for q in range(PARTS):
                 result_copy(which, k, q).wait_recv()
-            finish_one(which, k, lambda q, e: ret[which * near + k, q, e], 0)
             return carry
 
-        lax.fori_loop(1, near, finish, 0)
+        lax.fori_loop(1, near, collect, 0)
 
     def drain(k, carry):
         id_copy(k, half).wait_send()
@@ -374,18 +396,16 @@
     bf16, f32 = jnp.bfloat16, jnp.float32
     dma = pltpu.SemaphoreType.DMA
     vmem, anywhere = pl.BlockSpec(memory_space=pltpu.VMEM), pl.BlockSpec(memory_space=pl.ANY)
-    out = pl.pallas_call(
+    mixed = pl.pallas_call(
         functools.partial(kernel, sp, dp),
-        out_shape=jax.ShapeDtypeStruct((tokens, width), bf16),
-        in_specs=[anywhere] * 6,
-        out_specs=vmem,
+        out_shape=jax.ShapeDtypeStruct((dp // per, PARTS, part, width), bf16),
+        in_specs=[anywhere] * 5,
+        out_specs=anywhere,
         scratch_shapes=[
-            pltpu.VMEM((tokens, width), bf16),
             pltpu.VMEM((tokens, width), bf16),
             pltpu.VMEM((1, tokens), jnp.int32),
             pltpu.VMEM((1, HEAD_DIM), bf16),
             pltpu.VMEM((1, block_len), bf16),
-            pltpu.VMEM((tokens, width), f32),
             pltpu.VMEM((2 * blocks, block_len, HEAD_DIM), bf16),
             pltpu.VMEM((2 * blocks, block_len, HEAD_DIM), bf16),
             pltpu.VMEM((blocks, per, 1, tokens), jnp.int32),
@@ -393,28 +413,29 @@
             pltpu.VMEM((blocks, block_len, LANES), bf16),
             pltpu.VMEM((2, block_len, block_len), bf16),
             pltpu.VMEM((2 * blocks, PARTS, dp, part, HEAD_DIM), bf16),
-            pltpu.VMEM((sp, PARTS, dp // per, part, HEAD_DIM), bf16),
             pltpu.VMEM((2, block_len, LANES), f32),
             pltpu.VMEM((1, block_len + HEAD_DIM), f32),
             pltpu.VMEM((1, block_len + HEAD_DIM), f32),
-            dma((5,)), dma((sp,)), dma((sp,)), dma((sp,)), dma((sp,)),
+            dma((4,)), dma((sp,)), dma((sp,)), dma((sp,)), dma((sp,)),
             dma((sp * PARTS,)), dma((sp * PARTS,)),
             dma((2 * dp * PARTS,)), dma((2 * planes * PARTS,)), dma((2 * PARTS,)),
             dma((2 * planes * PARTS,)), dma, dma((PARTS,)), dma, dma,
-            pltpu.SemaphoreType.REGULAR,
+            pltpu.SemaphoreType.REGULAR, dma((2 * PARTS,)),
         ],
         compiler_params=pltpu.CompilerParams(
-            collective_id=0, has_side_effects=True, vmem_limit_bytes=60 * 1024 * 1024
+            collective_id=0, has_side_effects=True, vmem_limit_bytes=48 * 1024 * 1024
         ),
     )(
-        value_in.reshape(tokens, width),
-        segments,
-        value_gain.reshape(1, HEAD_DIM),
-        mixing.reshape(rows, block_len),
-        mixing_bias,
-        gate_in.reshape(tokens, width),
+        *[pltpu.with_memory_space_constraint(array, pltpu.HBM) for array in (
+            value_in.reshape(tokens, width),
+            segments,
+            value_gain.reshape(1, HEAD_DIM),
+            mixing.reshape(rows, block_len),
+            mixing_bias,
+        )]
     )
-    return out.reshape(sequences, tokens, width)
+    gated = gelu(gate_in.astype(f32)) * mixed.reshape(sequences, tokens, width).astype(f32)
+    return gated.astype(bf16)
 
 
 def solution(mesh):

time: 47.5 us -> 45.6 us (0.960)
  local copies, waits for them, and re-layouts: 2.26 us -> 0.01 us
  other arithmetic: 0 us -> 1.83 us
  Pallas kernels: 45 us -> 43.6 us
    unnamed x1 -> x2, local copies, waits for them, and re-layouts: 2.26 us -> 0.01 us
    convert_element_type x0 -> x1, other arithmetic: none -> 1.83 us  [per_device(): return gated.astype(bf16)]
    pallas_call x1, Pallas kernels: 45 us -> 43.6 us  [per_device(): pl.pallas_call(functools.partial(kernel, sp, dp), out_shape=jax.ShapeDtyp...]
where the time goes in v3:
time: 45.6 us; the launch traced here: 45.4 us
  Pallas kernels  43.6 us (96%)
  other arithmetic  1.83 us (4%)
    pallas_call x1, Pallas kernels, per_device(): pl.pallas_call(functools.partial(kernel, sp, dp), out_shape=jax.ShapeDtyp...  43.6 us
    convert_element_type x1, other arithmetic, per_device(): return gated.astype(bf16)  1.83 us

profile of v3, /device:TPU:0, one launch (start us, length us, event | category | flops | bytes accessed | tf_op | source)
XLA Modules:
  0.0 45.4 jit_solution(8742857165543080897)
XLA Ops:
  0.0 0.0 copy-start
  0.0 43.6 %shard_map.64 = bf16[2,4,64,1024]{3,2,1,0:T(8,128)(2,1)S(1)} custom-call(bf16[512,1024]{1,0:T(8,128)(2,1)} %bitcast.6, s32[1,512]{1,0:T(1,128)} %ids_hbm.1, bf16[1,128]{1,0:T(2,128)(2,1)} %bitcast.8, bf16[256,1024]{1,0:T(8,128)(2,1)} %bitcast.7, bf16[1,1024]{1,0:T(2,128)(2,1)} %bias_hbm.1), custom_call_target="tpu_custom_call" | custom-call | tf_op jit(solution)/shard_map/pallas_call | solution.py:399
  43.6 0.0 copy-done
  43.6 1.8 %fusion.6 = bf16[1,512,1024]{2,1,0:T(8,128)(2,1)} fusion(bf16[1,512,1024]{2,1,0:T(8,128)(2,1)S(1)} %copy-done, bf16[1,512,1024]{2,1,0:T(8,128)(2,1)S(1)} %bitcast.5), kind=kLoop, calls=%fused_computation.10 | loop fusion | flops 6291456 | bytes 3145728 | tf_op jit(solution)/shard_map/convert_element_type | solution.py:438
Async XLA Ops:
  0.0 43.6 %copy-start = (bf16[1,512,1024]{2,1,0:T(8,128)(2,1)S(1)}, bf16[1,512,1024]{2,1,0:T(8,128)(2,1)}, u32[]{:S(2)}) copy-start(bf16[1,512,1024]{2,1,0:T(8,128)(2,1)} %param.6) | copy-start | bytes 3145732

commit v4 on v3

--- a/solution.py
+++ b/solution.py
@@ -11,7 +11,12 @@
 CORES = 2
 LANES = 128
 ROW_STEP = 256
-PARTS = 4
+UNITS = 8
+NEAR_PARTS = 4
+FAR_SPLIT = ((0, 2), (2, 2), (4, 2), (6, 2))
+PARTS = len(FAR_SPLIT)
+AHEAD = 2
+LAG = 1
 MESH = pl.DeviceIdType.MESH
 
 epsilon = 1e-06
@@ -38,11 +43,11 @@
 
 
 def kernel(
-    sp, dp, value_hbm, ids_hbm, gain_hbm, mixing_ref, bias_hbm, mixed_ref,
-    value_ref, ids_ref, gain_ref, bias_ref,
-    vals, normed, ids, ids_row, ids_col, mix, res, bias_col, extras, extras_in,
+    sp, dp, value_hbm, ids_hbm, gain_hbm, mixing_ref, bias_hbm, gate_hbm, mixed_ref, act_hbm,
+    value_ref, ids_ref, gain_ref, bias_ref, gate_ref,
+    act_gate, vals, normed, ids, ids_row, ids_col, mix, res, bias_col, extras, extras_in,
     in_sem, v_send, v_recv, i_send, i_recv, r_send, r_recv,
-    mix_recv, across_send, core_send, fwd_send, own_sem, far_send, e_send, e_recv, far_ok, keep_sem,
+    mix_recv, across_send, core_send, fwd_send, own_sem, far_send, e_send, e_recv, far_ok, keep_sem, act_sem,
 ):
     s, d = lax.axis_index("sp"), lax.axis_index("dp")
     tokens = value_ref.shape[0]
@@ -51,7 +56,7 @@
     near = sp // 2
     blocks = near // per
     rows = mixing_ref.shape[0]
-    part = rows // PARTS
+    unit = rows // UNITS
     planes = dp // CORES
     half = s % per
     partner = d + 1 - 2 * (d % CORES)
@@ -80,7 +85,7 @@
         pltpu.make_async_copy(src, dst, in_sem.at[n])
         for n, (src, dst) in enumerate([
             (value_hbm, value_ref), (ids_hbm, ids_ref), (gain_hbm, gain_ref),
-            (bias_hbm, bias_ref),
+            (bias_hbm, bias_ref), (gate_hbm, gate_ref),
         ])
     ]
     for load in loads:
@@ -88,9 +93,19 @@
 
     count = (1, PARTS)
 
+    def span(which, q):
+        if which:
+            return FAR_SPLIT[q]
+        return q * (UNITS // NEAR_PARTS), UNITS // NEAR_PARTS
+
+    def rows_of(which, origin, q):
+        first, units = span(which, q)
+        return pl.ds(pl.multiple_of(origin * rows + first * unit, unit), units * unit)
+
     def chunk(which, origin, q):
-        size = rows // count[which]
-        return mix.at[which, pl.ds(pl.multiple_of(origin * rows + q * size, size), size)]
+        if which:
+            return mix.at[1, rows_of(1, origin, q)]
+        return mix.at[0, pl.ds(pl.multiple_of(origin * rows, rows), rows)]
 
     def part_copy(which, src, origin, q, where, sem):
         return pltpu.make_async_remote_copy(
@@ -103,7 +118,7 @@
         return chunk(1, d, q) if which else mixing_ref
 
     def from_far(q):
-        return part_copy(1, mixing_ref.at[pl.ds(q * part, part)], d, q, {"sp": far}, far_send.at[q])
+        return part_copy(1, mixing_ref.at[rows_of(1, 0, q)], d, q, {"sp": far}, far_send.at[q])
 
     def to_plane(which, step, q):
         sem = across_send.at[(which * planes + step) * PARTS + q]
@@ -163,11 +178,14 @@
         )
 
     def place(owner, which, q):
-        return mixed_ref.at[:, q, :, lanes_of(head_of(owner, which))]
+        return mixed_ref.at[:, pl.ds(*span(which, q)), :, lanes_of(head_of(owner, which))]
+
+    def slab(which, block, end, q):
+        return res.at[which * blocks + block, pl.ds(end * each, each), pl.ds(*span(which, q))]
 
     def keep_copy(which, q):
         return pltpu.make_async_copy(
-            res.at[which * blocks, q, pl.ds(half * each, each)],
+            slab(which, 0, half, q),
             place(s, which, q), keep_sem.at[which * PARTS + q],
         )
 
@@ -175,7 +193,7 @@
         target = flip(s, k, sp)
         at = (which * near + k) * PARTS + q
         return pltpu.make_async_remote_copy(
-            src_ref=res.at[which * blocks + k // per, q, pl.ds((target % per) * each, each)],
+            src_ref=slab(which, k // per, target % per, q),
             dst_ref=place(s, which, q),
             send_sem=r_send.at[at], recv_sem=r_recv.at[at],
             device_id={"sp": target}, device_id_type=MESH,
@@ -268,19 +286,21 @@
             right = normed[n]
             tall = []
             for origin in range(dp):
-                at = origin * rows + q * part
-                col = ids_col[j, pl.ds(pl.multiple_of(at, part), part), :]
+                at = rows_of(which, origin, q)
+                col = ids_col[j, at, :]
                 wide = []
                 for c in range(0, block_len, LANES):
                     same = col == row_b[:, c : c + LANES]
-                    piece = mix[which, pl.ds(pl.multiple_of(at, part), part), c : c + LANES]
+                    piece = mix[which, at, c : c + LANES]
                     wide.append(jnp.where(same, piece, zero))
                 tall.append(jnp.concatenate(wide, axis=1))
             summed = jnp.dot(jnp.concatenate(tall, axis=0), right, preferred_element_type=jnp.float32)
+            first, units = span(which, q)
+            tile = units * unit
             for origin in range(dp):
-                at = origin * rows + q * part
-                bias = bias_col[which, pl.ds(pl.multiple_of(at, part), part), :]
-                res[n, q, origin] = (summed[origin * part : (origin + 1) * part] + bias).astype(jnp.bfloat16)
+                bias = bias_col[which, rows_of(which, origin, q), :]
+                ready = (summed[origin * tile : (origin + 1) * tile] + bias).astype(jnp.bfloat16)
+                res[n, origin, pl.ds(first, units)] = ready.reshape(units, unit, HEAD_DIM)
             for i in range(per):
                 k = j * per + i
 
@@ -296,6 +316,16 @@
         lax.fori_loop(0, last - first, body, 0)
 
     norm_blocks(0, 0, blocks)
+    loads[4].wait()
+
+    def gate_rows(n, carry):
+        at = pl.ds(pl.multiple_of(n * LANES, LANES), LANES)
+        act_gate[at, :] = gelu(gate_ref[at, :].astype(jnp.float32))
+        return carry
+
+    lax.fori_loop(0, tokens // LANES, gate_rows, 0)
+    act_copy = pltpu.make_async_copy(act_gate, act_hbm, act_sem)
+    act_copy.start()
 
     def relay(q):
         from_far(q).wait_recv()
@@ -306,7 +336,7 @@
             mix_part(0, q, first, last)
             return carry
 
-        lax.fori_loop(0, PARTS, body, 0)
+        lax.fori_loop(0, NEAR_PARTS, body, 0)
 
     def near_here():
         forward(0, 0)
@@ -325,39 +355,39 @@
 
     @pl.when(mid)
     def _():
-        relay(0)
-        relay(1)
+        for q in range(AHEAD):
+            relay(q)
         near_here()
-        far_values()
         for q in range(PARTS):
             forward(1, q)
-            if q + 2 < PARTS:
-                relay(q + 2)
-            if q > 0:
+            if q + AHEAD < PARTS:
+                relay(q + AHEAD)
+            if q == 0:
+                far_values()
+            else:
                 far_part(q - 1)
         far_part(PARTS - 1)
 
     @pl.when(outer)
     def _():
         near_here()
-        relay(0)
-        far_values()
-        relay(1)
-        forward(1, 0)
-        for q in range(2, PARTS):
-            relay(q)
-            forward(1, q - 1)
-            far_part(q - 2)
-        far_part(PARTS - 2)
-        forward(1, PARTS - 1)
+        for n in range(PARTS + LAG):
+            if n < PARTS:
+                relay(n)
+            if n == LAG:
+                far_values()
+            if n > LAG:
+                far_part(n - LAG - 1)
+            if n >= LAG:
+                forward(1, n - LAG)
         far_part(PARTS - 1)
 
     for which in (0, 1):
-        for q in range(PARTS):
+        for q in range((NEAR_PARTS, PARTS)[which]):
             keep_copy(which, q).wait()
 
         def collect(k, carry):
-            for q in range(PARTS):
+            for q in range((NEAR_PARTS, PARTS)[which]):
                 result_copy(which, k, q).wait_recv()
             return carry
 
@@ -367,11 +397,12 @@
         id_copy(k, half).wait_send()
         for which in (0, 1):
             value_copy(which, k, half).wait_send()
-            for q in range(PARTS):
+            for q in range((NEAR_PARTS, PARTS)[which]):
                 result_copy(which, k, q).wait_send()
         return carry
 
     lax.fori_loop(1, near, drain, 0)
+    act_copy.wait()
     extras_copy().wait_send()
     for q in range(PARTS):
         from_far(q).wait_send()
@@ -392,38 +423,43 @@
     near = sp // 2
     blocks = near // per
     planes = dp // CORES
-    part = rows // PARTS
+    unit = rows // UNITS
     bf16, f32 = jnp.bfloat16, jnp.float32
     dma = pltpu.SemaphoreType.DMA
     vmem, anywhere = pl.BlockSpec(memory_space=pltpu.VMEM), pl.BlockSpec(memory_space=pl.ANY)
-    mixed = pl.pallas_call(
+    mixed, act = pl.pallas_call(
         functools.partial(kernel, sp, dp),
-        out_shape=jax.ShapeDtypeStruct((dp // per, PARTS, part, width), bf16),
-        in_specs=[anywhere] * 5,
-        out_specs=anywhere,
+        out_shape=(
+            jax.ShapeDtypeStruct((dp // per, UNITS, unit, width), bf16),
+            jax.ShapeDtypeStruct((tokens, width), f32),
+        ),
+        in_specs=[anywhere] * 6,
+        out_specs=(anywhere, anywhere),
         scratch_shapes=[
             pltpu.VMEM((tokens, width), bf16),
             pltpu.VMEM((1, tokens), jnp.int32),
             pltpu.VMEM((1, HEAD_DIM), bf16),
             pltpu.VMEM((1, block_len), bf16),
+            pltpu.VMEM((tokens, width), bf16),
+            pltpu.VMEM((tokens, width), f32),
             pltpu.VMEM((2 * blocks, block_len, HEAD_DIM), bf16),
             pltpu.VMEM((2 * blocks, block_len, HEAD_DIM), bf16),
             pltpu.VMEM((blocks, per, 1, tokens), jnp.int32),
             pltpu.VMEM((blocks, 1, block_len), f32),
             pltpu.VMEM((blocks, block_len, LANES), bf16),
             pltpu.VMEM((2, block_len, block_len), bf16),
-            pltpu.VMEM((2 * blocks, PARTS, dp, part, HEAD_DIM), bf16),
+            pltpu.VMEM((2 * blocks, dp, UNITS, unit, HEAD_DIM), bf16),
             pltpu.VMEM((2, block_len, LANES), f32),
             pltpu.VMEM((1, block_len + HEAD_DIM), f32),
             pltpu.VMEM((1, block_len + HEAD_DIM), f32),
-            dma((4,)), dma((sp,)), dma((sp,)), dma((sp,)), dma((sp,)),
+            dma((5,)), dma((sp,)), dma((sp,)), dma((sp,)), dma((sp,)),
             dma((sp * PARTS,)), dma((sp * PARTS,)),
             dma((2 * dp * PARTS,)), dma((2 * planes * PARTS,)), dma((2 * PARTS,)),
             dma((2 * planes * PARTS,)), dma, dma((PARTS,)), dma, dma,
-            pltpu.SemaphoreType.REGULAR, dma((2 * PARTS,)),
+            pltpu.SemaphoreType.REGULAR, dma((2 * PARTS,)), dma,
         ],
         compiler_params=pltpu.CompilerParams(
-            collective_id=0, has_side_effects=True, vmem_limit_bytes=48 * 1024 * 1024
+            collective_id=0, has_side_effects=True, vmem_limit_bytes=44 * 1024 * 1024
         ),
     )(
         *[pltpu.with_memory_space_constraint(array, pltpu.HBM) for array in (
@@ -432,10 +468,11 @@
             value_gain.reshape(1, HEAD_DIM),
             mixing.reshape(rows, block_len),
             mixing_bias,
+            gate_in.reshape(tokens, width),
         )]
     )
-    gated = gelu(gate_in.astype(f32)) * mixed.reshape(sequences, tokens, width).astype(f32)
-    return gated.astype(bf16)
+    gated = act * mixed.reshape(tokens, width).astype(f32)
+    return gated.astype(bf16).reshape(sequences, tokens, width)
 
 
 def solution(mesh):

time: 45.6 us -> 45 us (0.987)
    convert_element_type x1 -> x0, other arithmetic: 1.83 us -> none  [per_device(): return gated.astype(bf16)]
    reshape x0 -> x1, other arithmetic: none -> 1.38 us  [per_device(): return gated.astype(bf16).reshape(sequences, tokens, width)]
where the time goes in v4:
time: 45 us; the launch traced here: 44.9 us
  Pallas kernels  43.5 us (97%)
  other arithmetic  1.38 us (3%)
    pallas_call x1, Pallas kernels, per_device(): pl.pallas_call(functools.partial(kernel, sp, dp), out_shape=(jax.ShapeDty...  43.5 us
    reshape x1, other arithmetic, per_device(): return gated.astype(bf16).reshape(sequences, tokens, width)  1.38 us

profile of v4, /device:TPU:0, one launch (start us, length us, event | category | flops | bytes accessed | tf_op | source)
XLA Modules:
  0.0 44.9 jit_solution(4729942435105174989)
XLA Ops:
  0.0 43.5 %shard_map.64 = (bf16[2,8,32,1024]{3,2,1,0:T(8,128)(2,1)S(1)}, f32[512,1024]{1,0:T(8,128)S(1)}) custom-call(bf16[512,1024]{1,0:T(8,128)(2,1)} %bitcast.9, s32[1,512]{1,0:T(1,128)} %ids_hbm.1, bf16[1,128]{1,0:T(2,128)(2,1)} %bitcast.12, bf16[256,1024]{1,0:T(8,128)(2,1)} %bitcast.11, bf16[1,1024]{1,0:T(2,128)(2,1)} %bias_hbm.1, bf16[512,1024]{1,0:T(8,128)(2,1)} %bitcast.10), custom_call_target="tpu_custom_call" | custom-call | tf_op jit(solution)/shard_map/pallas_call | solution.py:430
  43.5 1.4 %fusion.1 = bf16[1,512,1024]{2,1,0:T(8,128)(2,1)} fusion(f32[512,1024]{1,0:T(8,128)S(1)} %get-tuple-element.7, bf16[2,8,32,1024]{3,2,1,0:T(8,128)(2,1)S(1)} %get-tuple-element.8), kind=kLoop, calls=%fused_computation.2 | loop fusion | flops 1572864 | bytes 4194304 | tf_op jit(solution)/shard_map/reshape | solution.py:475

commit v5 on v4

--- a/solution.py
+++ b/solution.py
@@ -12,10 +12,10 @@
 LANES = 128
 ROW_STEP = 256
 UNITS = 8
-NEAR_PARTS = 4
+NEAR_PARTS = 2
 FAR_SPLIT = ((0, 2), (2, 2), (4, 2), (6, 2))
 PARTS = len(FAR_SPLIT)
-AHEAD = 2
+AHEAD = 3
 LAG = 1
 MESH = pl.DeviceIdType.MESH
 
@@ -278,9 +278,11 @@
 
     zero = jnp.zeros((), jnp.bfloat16)
 
-    def mix_part(which, q, first=0, last=blocks):
+    def mix_part(which, q, first=0, last=blocks, up=False):
+        begin = first
+
         def body(m, carry):
-            j = last - 1 - m
+            j = begin + m if up else last - 1 - m
             n = which * blocks + j
             row_b = ids_row[j].astype(jnp.bfloat16)
             right = normed[n]
@@ -349,9 +351,9 @@
         bias_col[1] = to_column(extras_in[:, :block_len])
         norm_blocks(1, 0, blocks)
 
-    def far_part(q):
+    def far_part(q, up=False):
         arrived(1, q)
-        mix_part(1, q)
+        mix_part(1, q, up=up)
 
     @pl.when(mid)
     def _():
@@ -377,10 +379,10 @@
             if n == LAG:
                 far_values()
             if n > LAG:
-                far_part(n - LAG - 1)
+                far_part(n - LAG - 1, True)
             if n >= LAG:
                 forward(1, n - LAG)
-        far_part(PARTS - 1)
+        far_part(PARTS - 1, True)
 
     for which in (0, 1):
         for q in range((NEAR_PARTS, PARTS)[which]):

time: 45 us -> 45.1 us (level)
  no operation moved by 1% of the time
where the time goes in v5:
time: 45.1 us; the launch traced here: 44.9 us
  Pallas kernels  43.5 us (96%)
  other arithmetic  1.38 us (3%)
    pallas_call x1, Pallas kernels, per_device(): pl.pallas_call(functools.partial(kernel, sp, dp), out_shape=(jax.ShapeDty...  43.5 us
    reshape x1, other arithmetic, per_device(): return gated.astype(bf16).reshape(sequences, tokens, width)  1.38 us

profile of v5, /device:TPU:0, one launch (start us, length us, event | category | flops | bytes accessed | tf_op | source)
XLA Modules:
  0.0 44.9 jit_solution(266626479381993419)
XLA Ops:
  0.0 43.5 %shard_map.64 = (bf16[2,8,32,1024]{3,2,1,0:T(8,128)(2,1)S(1)}, f32[512,1024]{1,0:T(8,128)S(1)}) custom-call(bf16[512,1024]{1,0:T(8,128)(2,1)} %bitcast.9, s32[1,512]{1,0:T(1,128)} %ids_hbm.1, bf16[1,128]{1,0:T(2,128)(2,1)} %bitcast.12, bf16[256,1024]{1,0:T(8,128)(2,1)} %bitcast.11, bf16[1,1024]{1,0:T(2,128)(2,1)} %bias_hbm.1, bf16[512,1024]{1,0:T(8,128)(2,1)} %bitcast.10), custom_call_target="tpu_custom_call" | custom-call | tf_op jit(solution)/shard_map/pallas_call | solution.py:432
  43.6 1.4 %fusion.1 = bf16[1,512,1024]{2,1,0:T(8,128)(2,1)} fusion(f32[512,1024]{1,0:T(8,128)S(1)} %get-tuple-element.7, bf16[2,8,32,1024]{3,2,1,0:T(8,128)(2,1)S(1)} %get-tuple-element.8), kind=kLoop, calls=%fused_computation.2 | loop fusion | flops 1572864 | bytes 4194304 | tf_op jit(solution)/shard_map/reshape | solution.py:477
